TPU v7x, 32 devices: a whole 2x2x4 slice. The times are simulated.
32 devices in a mesh: grp: 2 (over x), kv: 4 (over z), tp: 4 (over y, core).
Axes of the slice: x: 2, y: 2, z: 4, core: 2. Of those that a mesh axis runs over, the one named last changes fastest.
Arguments:
- x_rows: bfloat16 [256, 4096], P('grp', 'kv'), parts along dimension 0, may hold values from -32 to 32
- in_gain: bfloat16 [4096], P('kv'), may hold values from 0.099609375 to 1.8984375
- query_weight: bfloat16 [4096, 4096], P('kv', 'tp'), may hold values from -0.09375 to 0.09375
- key_weight: bfloat16 [4096, 4096], P('kv', 'tp'), may hold values from -0.09375 to 0.09375
- value_weight: bfloat16 [4096, 8192], P('kv', 'tp'), may hold values from -0.09375 to 0.09375
- outgate_weight: bfloat16 [4096, 8192], P('kv', 'tp'), may hold values from -0.09375 to 0.09375
- input_gate_weight: bfloat16 [4096, 32], P('kv', 'tp'), may hold values from -0.09375 to 0.09375
- forget_gate_weight: bfloat16 [4096, 32], P('kv', 'tp'), may hold values from -0.09375 to 0.09375
- forget_bias: float32 [32], P('tp'), may hold values from -1 to 3
- state_matrix: float32 [256, 32, 128, 256], P(('grp', 'kv'), 'tp'), parts along dimension 0, may hold values from -3 to 3
- state_norm: float32 [256, 32, 128], P(('grp', 'kv'), 'tp'), parts along dimension 0, may hold values from -6 to 6
- state_max: float32 [256, 32], P(('grp', 'kv'), 'tp'), parts along dimension 0, may hold values from -1 to 1
- head_gain: bfloat16 [8192], P('tp'), may hold values from 0.099609375 to 1.8984375
- out_weight: bfloat16 [8192, 4096], P('tp', 'kv'), may hold values from -0.0625 to 0.0625
- mix_gain: bfloat16 [4096], P('kv'), may hold values from 0.099609375 to 1.8984375
- up_weight: bfloat16 [4096, 16384], P('kv', 'tp'), may hold values from -0.09375 to 0.09375
- down_weight: bfloat16 [16384, 4096], P('tp', 'kv'), may hold values from -0.046875 to 0.046875
Outputs:
- mixed_out: bfloat16 [256, 4096], P('grp', 'kv'), parts along dimension 0
- new_matrix: float32 [256, 32, 128, 256], P(('grp', 'kv'), 'tp'), parts along dimension 0
- new_norm: float32 [256, 32, 128], P(('grp', 'kv'), 'tp'), parts along dimension 0
- new_max: float32 [256, 32], P(('grp', 'kv'), 'tp'), parts along dimension 0
There are 2 independent parts, one for each index of `grp`. A program takes and returns all parts, laid end to end along the dimension named above; an argument that names none is the same for every part. Nothing has to cross between parts.
All inputs are finite; a program needn't handle non-finite values.
Results may differ from a plain program's by a relative error of at most 0.019.
Values may be sent and summed in bfloat16 or wider, within the bound.
A program may use at most 192 MiB of HBM per device.

v0:
```python
import functools
import math

import jax
import jax.numpy as jnp
from jax import lax
from jax.experimental import pallas as pl
from jax.experimental.pallas import tpu as pltpu
from jax.sharding import PartitionSpec as P

LANES = 128
EPS = 1e-06
MESH = pl.DeviceIdType.MESH
F32 = jnp.float32
BF16 = jnp.bfloat16


def kernel(
    kvn,
    tpn,
    width,
    model,
    x_ref,
    x3_ref,
    gain_ref,
    q_hbm,
    k_hbm,
    v_hbm,
    o_hbm,
    gate_ref,
    bias_ref,
    state_hbm,
    norm_ref,
    max_ref,
    head_gain_ref,
    out_hbm,
    mix_gain_ref,
    up_hbm,
    down_hbm,
    mixed_ref,
    matrix_hbm,
    new_norm_ref,
    new_max_ref,
    weights,
    down_w,
    state,
    scaled,
    part,
    gate_send,
    gate_recv,
    proj_send,
    proj_recv,
    q_all,
    k_all,
    v_all,
    o_all,
    fd_all,
    id_all,
    em_all,
    merged,
    merged_all,
    branch_send,
    branch_recv,
    resid_all,
    sq_send,
    sq_recv,
    up_send,
    up_recv,
    hidden_all,
    mix_send,
    mix_recv,
    mixed_all,
    w_sem,
    w2_sem,
    down_sem,
    state_sem,
    write_sem,
    gate_ss,
    gate_rs,
    proj_ss,
    proj_rs,
    mg_ss,
    mg_rs,
    br_ss,
    br_rs,
    rd_ss,
    rd_rs,
    sq_ss,
    sq_rs,
    up_ss,
    up_rs,
    hd_ss,
    hd_rs,
    mx_ss,
    mx_rs,
    ma_ss,
    ma_rs,
):
    me = lax.axis_index("kv")
    tme = lax.axis_index("tp")
    total, local = x_ref.shape
    rows, heads, dqk = norm_ref.shape
    dv = head_gain_ref.shape[1]
    trows = total // tpn
    tile = min(256, width)
    hidden_units = up_hbm.shape[1]

    def kv_peer(j):
        return lax.rem(me + j, kvn)

    def tp_peer(j):
        return lax.rem(tme + j, tpn)

    def send(src, dst, ssem, rsem, axis, peer):
        copy = pltpu.make_async_remote_copy(
            src_ref=src,
            dst_ref=dst,
            send_sem=ssem,
            recv_sem=rsem,
            device_id={axis: peer},
            device_id_type=MESH,
        )
        copy.start()
        return copy

    sent = []

    first = []
    for name, ref in enumerate((q_hbm, k_hbm, v_hbm, o_hbm)):
        for offset in range(0, ref.shape[1], width):
            first.append((name, ref, offset))
    loads = []
    for c, (name, ref, offset) in enumerate(first):
        copy = pltpu.make_async_copy(
            ref.at[:, pl.ds(offset, width)], weights.at[c], w_sem.at[c]
        )
        copy.start()
        loads.append(copy)
    second = []
    for a in range(0, out_hbm.shape[0], local):
        for b in range(0, out_hbm.shape[1], width):
            second.append((out_hbm, a, b))
    out_blocks = len(second)
    for b in range(0, hidden_units, width):
        second.append((up_hbm, 0, b))

    barrier = pltpu.get_barrier_semaphore()
    for j in range(1, kvn):
        pl.semaphore_signal(barrier, inc=1, device_id={"kv": kv_peer(j)}, device_id_type=MESH)
    for j in range(1, tpn):
        pl.semaphore_signal(barrier, inc=1, device_id={"tp": tp_peer(j)}, device_id_type=MESH)

    xf = x_ref[...].astype(F32)
    squares = jnp.sum(xf * xf, axis=1, keepdims=True)
    scaled[...] = (xf * gain_ref[...].astype(F32)).astype(BF16)
    gates = jnp.dot(scaled[...], gate_ref[...], preferred_element_type=F32)
    gate_send[:, :, 0 : 2 * LANES] = gates.reshape(kvn, rows, 2 * LANES)
    gate_send[:, :, 2 * LANES :] = jnp.broadcast_to(squares, (total, LANES)).reshape(
        kvn, rows, LANES
    )
    pl.semaphore_wait(barrier, (kvn - 1) + (tpn - 1))
    gate_copies = []
    for j in range(1, kvn):
        gate_copies.append(
            send(gate_send.at[kv_peer(j)], gate_recv.at[j - 1], gate_ss.at[j - 1], gate_rs.at[j - 1], "kv", kv_peer(j))
        )
    sent += gate_copies

    def matmul_chunk(lhs, slot, dest, c):
        def body(i, carry):
            cols = pl.ds(pl.multiple_of(i * tile, tile), tile)
            res = jnp.dot(lhs[...], weights[slot, :, cols], preferred_element_type=F32)
            dest[c, :, :, cols] = res.reshape(kvn, rows, tile).astype(BF16)
            return carry

        lax.fori_loop(0, width // tile, body, 0)

    def state_load(r):
        return pltpu.make_async_copy(state_hbm.at[r], state.at[r], state_sem.at[r])

    def state_store(r):
        return pltpu.make_async_copy(state.at[r], matrix_hbm.at[r], write_sem.at[r])

    proj_copies = []
    loads2 = []
    for c in range(len(first)):
        loads[c].wait()
        matmul_chunk(scaled, c, proj_send, c)
        for j in range(1, kvn):
            proj_copies.append(
                send(
                    proj_send.at[c, kv_peer(j)],
                    proj_recv.at[c, j - 1],
                    proj_ss.at[c, j - 1],
                    proj_rs.at[c, j - 1],
                    "kv",
                    kv_peer(j),
                )
            )
    sent += proj_copies
    for r in range(rows):
        state_load(r).start()
    for c, (ref, a, b) in enumerate(second):
        copy = pltpu.make_async_copy(
            ref.at[pl.ds(a, local), pl.ds(b, width)], weights.at[c], w2_sem.at[c]
        )
        copy.start()
        loads2.append(copy)
    down_load = pltpu.make_async_copy(down_hbm, down_w, down_sem.at[0])
    down_load.start()

    for copy in gate_copies:
        copy.wait_recv()
    gsum = gate_send[me]
    for j in range(1, kvn):
        gsum = gsum + gate_recv[j - 1]
    scale = lax.rsqrt(gsum[:, 2 * LANES : 2 * LANES + 1] / model + EPS)
    igate = gsum[:, 0:heads] * scale
    z = gsum[:, LANES : LANES + heads] * scale + bias_ref[...]
    logf = jnp.minimum(z, 0.0) - jnp.log1p(jnp.exp(-jnp.abs(z)))
    held = logf + max_ref[...]
    new_max = jnp.maximum(held, igate)
    new_max_ref[...] = new_max
    fdec = jnp.exp(held - new_max)
    idec = jnp.exp(igate - new_max)
    floor = jnp.exp(-new_max)
    for h in range(heads):
        for src, dst in ((fdec, fd_all), (idec, id_all), (floor, em_all)):
            dst[:, h, :] = jnp.broadcast_to(src[:, h : h + 1], (rows, LANES))

    targets = ((q_all, dqk), (k_all, dqk), (v_all, dv), (o_all, dv))
    for c, (name, ref, offset) in enumerate(first):
        for j in range(1, kvn):
            proj_copies[c * (kvn - 1) + j - 1].wait_recv()
        dst, extent = targets[name]
        for g in range(0, width, LANES):
            val = proj_send[c, me, :, g : g + LANES].astype(F32)
            for j in range(1, kvn):
                val = val + proj_recv[c, j - 1, :, g : g + LANES].astype(F32)
            val = (val * scale).astype(BF16).astype(F32)
            if name == 0:
                val = val * (dqk ** (-0.5))
            at = offset + g
            col = at % extent
            dst[:, at // extent, col : col + LANES] = val

    pad = jnp.zeros((LANES - 2 * heads, dqk), F32)

    def row_body(r, carry):
        state_load(r).wait()
        q8, k8, v8, o8 = q_all[r], k_all[r], v_all[r], o_all[r]
        fd8, id8, em8 = fd_all[r], id_all[r], em_all[r]
        ik8 = id8 * k8
        turned = jnp.concatenate([ik8, q8, pad], axis=0).T
        numer = []
        for h in range(heads):
            fd = jnp.concatenate([fd8[h : h + 1, :]] * (dv // LANES), axis=1)
            new = fd * state[r, h] + turned[:, h : h + 1] * v8[h : h + 1, :]
            state[r, h] = new
            numer.append(
                jnp.sum(turned[:, heads + h : heads + h + 1] * new, axis=0, keepdims=True)
            )
        state_store(r).start()
        numer = jnp.concatenate(numer, axis=0)
        nn = fd8 * norm_ref[r] + ik8
        new_norm_ref[r] = nn
        denom = jnp.sum(q8 * nn, axis=1, keepdims=True)
        readout = numer / jnp.maximum(jnp.abs(denom), em8[:, 0:1])
        normed = readout * lax.rsqrt(
            jnp.sum(readout * readout, axis=1, keepdims=True) / dv + EPS
        )
        merged[r] = jax.nn.sigmoid(o8) * (normed * head_gain_ref[...])
        return carry

    lax.fori_loop(0, rows, row_body, 0)

    for h in range(heads):
        merged_all[me, :, h * dv : (h + 1) * dv] = merged[:, h, :].astype(BF16)
    mg = []
    for j in range(1, kvn):
        mg.append(
            send(merged_all.at[me], merged_all.at[me], mg_ss.at[j - 1], mg_rs.at[j - 1], "kv", kv_peer(j))
        )
    sent += mg
    for c in range(out_blocks):
        loads2[c].wait()
    for copy in mg:
        copy.wait_recv()
    for b in range(0, local, width):

        def out_body(i, carry, b=b):
            cols = pl.ds(pl.multiple_of(i * tile, tile), tile)
            acc = jnp.zeros((total, tile), F32)
            for c in range(out_blocks):
                _, a, bb = second[c]
                if bb != b:
                    continue
                lhs = merged_all[:, :, a : a + local].reshape(total, local)
                acc = acc + jnp.dot(lhs, weights[c, :, cols], preferred_element_type=F32)
            part[:, pl.ds(pl.multiple_of(b + i * tile, tile), tile)] = acc
            return carry

        lax.fori_loop(0, width // tile, out_body, 0)

    def reduce_tp(buf_send, buf_recv, ssem, rsem):
        for j in range(tpn):
            buf_send[j] = part[j * trows : (j + 1) * trows, :].astype(BF16)
        copies = []
        for j in range(1, tpn):
            copies.append(
                send(buf_send.at[tp_peer(j)], buf_recv.at[j - 1], ssem.at[j - 1], rsem.at[j - 1], "tp", tp_peer(j))
            )
        for copy in copies:
            copy.wait_recv()
        val = buf_send[tme].astype(F32)
        for j in range(1, tpn):
            val = val + buf_recv[j - 1].astype(F32)
        return val, copies

    def gather_tp(buf, ssem, rsem):
        copies = []
        for j in range(1, tpn):
            copies.append(
                send(buf.at[tme], buf.at[tme], ssem.at[j - 1], rsem.at[j - 1], "tp", tp_peer(j))
            )
        for copy in copies:
            copy.wait_recv()
        return copies

    branch, copies = reduce_tp(branch_send, branch_recv, br_ss, br_rs)
    sent += copies
    resid_all[tme] = (x3_ref[tme].astype(F32) + branch).astype(BF16)
    sent += gather_tp(resid_all, rd_ss, rd_rs)

    for j in range(tpn):
        part[j * trows : (j + 1) * trows, :] = resid_all[j].astype(F32)
    rf = part[...]
    sq = jnp.sum(rf * rf, axis=1, keepdims=True)
    scaled[...] = (rf * mix_gain_ref[...].astype(F32)).astype(BF16)
    sq_send[...] = jnp.broadcast_to(sq, (total, LANES)).reshape(kvn, rows, LANES)
    sq_copies = []
    for j in range(1, kvn):
        sq_copies.append(
            send(sq_send.at[kv_peer(j)], sq_recv.at[j - 1], sq_ss.at[j - 1], sq_rs.at[j - 1], "kv", kv_peer(j))
        )
    sent += sq_copies
    chunks = hidden_units // width
    up_copies = []
    for c in range(chunks):
        loads2[out_blocks + c].wait()
        matmul_chunk(scaled, out_blocks + c, up_send, c)
        for j in range(1, kvn):
            up_copies.append(
                send(
                    up_send.at[c, kv_peer(j)],
                    up_recv.at[c, j - 1],
                    up_ss.at[c, j - 1],
                    up_rs.at[c, j - 1],
                    "kv",
                    kv_peer(j),
                )
            )
    sent += up_copies
    for copy in sq_copies:
        copy.wait_recv()
    sq_sum = sq_send[me]
    for j in range(1, kvn):
        sq_sum = sq_sum + sq_recv[j - 1]
    scale_two = lax.rsqrt(sq_sum[:, 0:1] / model + EPS)
    hidden_copies = []
    for c in range(chunks):
        for j in range(1, kvn):
            up_copies[c * (kvn - 1) + j - 1].wait_recv()
        val = up_send[c, me].astype(F32)
        for j in range(1, kvn):
            val = val + up_recv[c, j - 1].astype(F32)
        act = jnp.maximum(val * scale_two, 0.0)
        hidden_all[c, me] = (act * act).astype(BF16)
        for j in range(1, kvn):
            hidden_copies.append(
                send(
                    hidden_all.at[c, me],
                    hidden_all.at[c, me],
                    hd_ss.at[c, j - 1],
                    hd_rs.at[c, j - 1],
                    "kv",
                    kv_peer(j),
                )
            )
    sent += hidden_copies
    down_load.wait()
    for c in range(chunks):
        for j in range(1, kvn):
            hidden_copies[c * (kvn - 1) + j - 1].wait_recv()

        def down_body(i, carry, c=c):
            cols = pl.ds(pl.multiple_of(i * tile, tile), tile)
            lhs = hidden_all[c].reshape(total, width)
            res = jnp.dot(
                lhs, down_w[c * width : (c + 1) * width, cols], preferred_element_type=F32
            )
            if c == 0:
                part[:, cols] = res
            else:
                part[:, cols] += res
            return carry

        lax.fori_loop(0, local // tile, down_body, 0)
    down, copies = reduce_tp(mix_send, mix_recv, mx_ss, mx_rs)
    sent += copies
    mixed_all[tme] = (resid_all[tme].astype(F32) + down).astype(BF16)
    sent += gather_tp(mixed_all, ma_ss, ma_rs)
    mixed_ref[...] = mixed_all[...]

    for copy in sent:
        copy.wait_send()

    def drain(r, carry):
        state_store(r).wait()
        return carry

    lax.fori_loop(0, rows, drain, 0)


def per_device(
    kvn,
    tpn,
    x_rows,
    in_gain,
    query_weight,
    key_weight,
    value_weight,
    outgate_weight,
    input_gate_weight,
    forget_gate_weight,
    forget_bias,
    state_matrix,
    state_norm,
    state_max,
    head_gain,
    out_weight,
    mix_gain,
    up_weight,
    down_weight,
):
    total, local = x_rows.shape
    rows, heads, dqk, dv = state_matrix.shape
    trows = total // tpn
    hidden_units = up_weight.shape[1]
    width = functools.reduce(
        math.gcd,
        [local, heads * dqk, heads * dv, hidden_units],
    )
    n_first = (2 * heads * dqk + 2 * heads * dv) // width
    n_second = (heads * dv // local) * (local // width) + hidden_units // width
    chunks = hidden_units // width
    gap = ((0, 0), (0, LANES - heads))
    gate = jnp.concatenate(
        [jnp.pad(input_gate_weight, gap), jnp.pad(forget_gate_weight, gap)], axis=1
    )
    vmem = pl.BlockSpec(memory_space=pltpu.VMEM)
    hbm = pl.BlockSpec(memory_space=pl.ANY)
    V = pltpu.VMEM
    dma = pltpu.SemaphoreType.DMA
    k1, t1 = max(kvn - 1, 1), max(tpn - 1, 1)
    scratch = [
        V((max(n_first, n_second), local, width), BF16),
        V((hidden_units, local), BF16),
        V((rows, heads, dqk, dv), F32),
        V((total, local), BF16),
        V((total, local), F32),
        V((kvn, rows, 3 * LANES), F32),
        V((k1, rows, 3 * LANES), F32),
        V((n_first, kvn, rows, width), BF16),
        V((n_first, k1, rows, width), BF16),
        V((rows, heads, dqk), F32),
        V((rows, heads, dqk), F32),
        V((rows, heads, dv), F32),
        V((rows, heads, dv), F32),
        V((rows, heads, LANES), F32),
        V((rows, heads, LANES), F32),
        V((rows, heads, LANES), F32),
        V((rows, heads, dv), F32),
        V((kvn, rows, heads * dv), BF16),
        V((tpn, trows, local), BF16),
        V((t1, trows, local), BF16),
        V((tpn, trows, local), BF16),
        V((kvn, rows, LANES), F32),
        V((k1, rows, LANES), F32),
        V((chunks, kvn, rows, width), BF16),
        V((chunks, k1, rows, width), BF16),
        V((chunks, kvn, rows, width), BF16),
        V((tpn, trows, local), BF16),
        V((t1, trows, local), BF16),
        V((tpn, trows, local), BF16),
        dma((n_first,)),
        dma((n_second,)),
        dma((1,)),
        dma((rows,)),
        dma((rows,)),
        dma((k1,)),
        dma((k1,)),
        dma((n_first, k1)),
        dma((n_first, k1)),
        dma((k1,)),
        dma((k1,)),
        dma((t1,)),
        dma((t1,)),
        dma((t1,)),
        dma((t1,)),
        dma((k1,)),
        dma((k1,)),
        dma((chunks, k1)),
        dma((chunks, k1)),
        dma((chunks, k1)),
        dma((chunks, k1)),
        dma((t1,)),
        dma((t1,)),
        dma((t1,)),
        dma((t1,)),
    ]
    model = local * kvn
    mixed, new_matrix, new_norm, new_max = pl.pallas_call(
        functools.partial(kernel, kvn, tpn, width, model),
        out_shape=(
            jax.ShapeDtypeStruct((tpn, trows, local), BF16),
            jax.ShapeDtypeStruct(state_matrix.shape, F32),
            jax.ShapeDtypeStruct(state_norm.shape, F32),
            jax.ShapeDtypeStruct(state_max.shape, F32),
        ),
        in_specs=[vmem, vmem, vmem, hbm, hbm, hbm, hbm, vmem, vmem, hbm, vmem, vmem, vmem, hbm, vmem, hbm, hbm],
        out_specs=(vmem, hbm, vmem, vmem),
        scratch_shapes=scratch,
        compiler_params=pltpu.CompilerParams(
            collective_id=0, has_side_effects=True, vmem_limit_bytes=67043328
        ),
    )(
        x_rows,
        x_rows.reshape(tpn, trows, local),
        in_gain.reshape(1, local),
        query_weight,
        key_weight,
        value_weight,
        outgate_weight,
        gate,
        forget_bias.reshape(1, heads),
        state_matrix,
        state_norm,
        state_max,
        head_gain.astype(F32).reshape(heads, dv),
        out_weight,
        mix_gain.reshape(1, local),
        up_weight,
        down_weight,
    )
    return (mixed.reshape(total, local), new_matrix, new_norm, new_max)


def solution(mesh):
    placed = (
        P("grp", "kv"),
        P("kv"),
        P("kv", "tp"),
        P("kv", "tp"),
        P("kv", "tp"),
        P("kv", "tp"),
        P("kv", "tp"),
        P("kv", "tp"),
        P("tp"),
        P(("grp", "kv"), "tp", None, None),
        P(("grp", "kv"), "tp", None),
        P(("grp", "kv"), "tp"),
        P("tp"),
        P("tp", "kv"),
        P("kv"),
        P("kv", "tp"),
        P("tp", "kv"),
    )
    return jax.shard_map(
        functools.partial(per_device, mesh.shape["kv"], mesh.shape["tp"]),
        mesh=mesh,
        in_specs=placed,
        out_specs=(
            P("grp", "kv"),
            P(("grp", "kv"), "tp", None, None),
            P(("grp", "kv"), "tp", None),
            P(("grp", "kv"), "tp"),
        ),
        check_vma=False,
    )
```

profile of v0, /device:TPU:0, one launch (start us, length us, event | category | flops | bytes accessed | tf_op | source)
XLA Modules:
  0.0 180.4 jit_solution(14133066658705827928)
XLA Ops:
  0.6 1.3 reshape.29.gain_ref
  1.9 1.3 reshape.33.mix_gain_ref
  3.2 1.3 reshape.36.head_gain_ref
  4.5 1.4 copy.23.max_ref
  5.8 0.9 copy.21
  6.7 0.9 copy.22
  7.6 0.9 fusion.2.gate_ref
  8.5 145.1 %shard_map.192 = (bf16[4,32,1024]{2,1,0:T(8,128)(2,1)}, f32[32,8,128,256]{3,2,1,0:T(8,128)}, f32[32,8,128]{2,1,0:T(8,128)}, f32[32,8]{1,0:T(8,128)}) custom-call(bf16[128,1024]{1,0:T(8,128)(2,1)} %x_ref.1, bf16[4,32,1024]{2,1,0:T(8,128)(2,1)} %bitcast.3, bf16[1,1024]{1,0:T(2,128)(2,1)} %reshape.29.gain_ref, bf16[1024,1024]{1,0:T(8,128)(2,1)} %q_hbm.1, ...), custom_call_target="tpu_custom_call" | custom-call | tf_op jit(solution)/shard_map/pallas_call | solution.py:523
  153.6 1.4 copy.24
  155.0 1.7 copy.28
  156.7 0.0 copy-start
  156.7 23.0 %copy.29 = f32[32,8,128,256]{3,2,1,0:T(8,128)} copy(f32[32,8,128,256]{3,2,1,0:T(8,128)} %get-tuple-element.21) | data formatting | bytes 67108864
  179.7 0.0 copy-done
  179.7 0.7 copy.30
Async XLA Ops:
  156.7 23.0 %copy-start = (f32[32,8,128]{2,1,0:T(8,128)S(1)}, f32[32,8,128]{2,1,0:T(8,128)}, u32[]{:S(2)}) copy-start(f32[32,8,128]{2,1,0:T(8,128)} %get-tuple-element.22) | copy-start | bytes 393220
where the time goes:
time: 181 us; the launch traced here: 180 us
  Pallas kernels  145 us (80%)
  local copies, waits for them, and re-layouts  33.7 us (19%)
    pallas_call x1, Pallas kernels, per_device(): pl.pallas_call(functools.partial(kernel, kvn, tpn, width, model), out_sha...  145 us
    unnamed x9, local copies, waits for them, and re-layouts  29.9 us

commit v1 on v0

v1 whole, which is shorter than its diff:
```python
import functools

import jax
import jax.numpy as jnp
from jax import lax
from jax.experimental import pallas as pl
from jax.experimental.pallas import tpu as pltpu
from jax.sharding import PartitionSpec as P

LANES = 128
EPS = 1e-06
MESH = pl.DeviceIdType.MESH
F32 = jnp.float32
BF16 = jnp.bfloat16
PIECES = 2
SKEW = 2
UP_SKEW = 3


def kernel(
    kvn,
    tpn,
    width,
    gate_heads,
    up_width,
    x_hbm,
    gain_hbm,
    q_hbm,
    k_hbm,
    v_hbm,
    o_hbm,
    ig_hbm,
    fg_hbm,
    bias_hbm,
    state_hbm,
    norm_hbm,
    max_hbm,
    head_gain_hbm,
    out_hbm,
    mix_gain_hbm,
    up_hbm,
    down_hbm,
    mixed_ref,
    state,
    new_norm_ref,
    new_max_ref,
    x_ref,
    gain_ref,
    ig_ref,
    fg_ref,
    bias_ref,
    norm_ref,
    max_ref,
    head_gain_ref,
    mix_gain_ref,
    weights,
    down_w,
    scaled,
    part,
    gate_send,
    gate_recv,
    max_pad,
    part_send,
    pair_recv,
    cross_recv,
    norm_h,
    fd_all,
    id_all,
    em_all,
    scale_b,
    hg_rows,
    numer_s,
    normed_all,
    merged_all,
    half_send,
    half_recv,
    y_send,
    y_recv,
    full,
    sq_send,
    sq_recv,
    scale_two,
    upb,
    up_cross,
    small_sem,
    w_sem,
    w2_sem,
    down_sem,
    state_sem,
    gate_ss,
    gate_rs,
    pair_ss,
    pair_rs,
    cross_ss,
    cross_rs,
    ag_ss,
    relay_ss,
    ag_rs,
    half_ss,
    half_rs,
    y_ss,
    y_rs,
    full_ss,
    full_rs,
    sq_ss,
    sq_rs,
    up_ss,
    up_rs,
    upx_ss,
    upx_rs,
    hid_ss,
    hid_rs,
):
    me = lax.axis_index("kv")
    tme = lax.axis_index("tp")
    total, local = x_ref.shape
    rows, heads, dqk = norm_ref.shape
    dv = v_hbm.shape[1] // heads
    model = local * kvn
    hidden_units = up_hbm.shape[1]
    hp = gate_send.shape[0] // 3
    gate_width = gate_heads * dv
    gate_chunks = heads // gate_heads
    chunks = heads + gate_chunks
    up_chunks = hidden_units // up_width
    npairs = kvn // 2
    pair = me // 2
    partner = me + 1 - 2 * (me % 2)
    lead_bit = 1 - (2 * pair) // npairs
    leader = (me % 2) == lead_bit
    outer = (me % 2) != lead_bit

    def wrap(j):
        return lax.rem(me + j, kvn)

    def remote(src, dst, ssem, rsem, axis, peer):
        return pltpu.make_async_remote_copy(
            src_ref=src,
            dst_ref=dst,
            send_sem=ssem,
            recv_sem=rsem,
            device_id={axis: peer},
            device_id_type=MESH,
        )

    def arrived(dst, rsem, ssem):
        remote(dst, dst, ssem, rsem, "kv", partner).wait_recv()

    def outside():
        for jj in range(1, npairs):
            other = lax.rem(pair + jj, npairs)
            for b in range(2):
                yield jj, b, 2 * other + b

    small = []
    for i, (src, dst) in enumerate(
        (
            (x_hbm, x_ref),
            (gain_hbm, gain_ref),
            (ig_hbm, ig_ref),
            (fg_hbm, fg_ref),
            (bias_hbm, bias_ref),
            (max_hbm, max_ref),
            (norm_hbm, norm_ref),
            (head_gain_hbm, head_gain_ref),
            (mix_gain_hbm, mix_gain_ref),
        )
    ):
        copy = pltpu.make_async_copy(src, dst, small_sem.at[i])
        copy.start()
        small.append(copy)

    def qkv_loads(h):
        found = []
        at = 0
        for i, (ref, extent) in enumerate(((q_hbm, dqk), (k_hbm, dqk), (v_hbm, dv))):
            src = ref.at[:, pl.ds(pl.multiple_of(h * extent, extent), extent)]
            found.append(pltpu.make_async_copy(src, weights.at[h, :, pl.ds(at, extent)], w_sem.at[h, i]))
            at += extent
        return found

    def gate_load(c):
        src = o_hbm.at[:, pl.ds(pl.multiple_of(c * gate_width, gate_width), gate_width)]
        return pltpu.make_async_copy(src, weights.at[heads + c, :, pl.ds(0, gate_width)], w_sem.at[heads + c, 0])

    for h in range(heads):
        for copy in qkv_loads(h):
            copy.start()
    for c in range(gate_chunks):
        gate_load(c).start()

    def state_load(h):
        return pltpu.make_async_copy(state_hbm.at[:, h], state.at[:, h], state_sem.at[h])

    for h in range(heads):
        state_load(h).start()

    tp_steps = []
    s = 1
    while s < tpn:
        tp_steps.append(s)
        s *= 2

    def tp_peer(s):
        return tme + s - 2 * s * ((tme // s) % 2)

    barrier = pltpu.get_barrier_semaphore()
    for j in range(1, kvn):
        pl.semaphore_signal(barrier, inc=1, device_id={"kv": wrap(j)}, device_id_type=MESH)
    for s in tp_steps:
        pl.semaphore_signal(barrier, inc=1, device_id={"tp": tp_peer(s)}, device_id_type=MESH)

    def row_of(ref):
        pieces = [ref[i : i + 1, :].astype(F32) for i in range(ref.shape[0])]
        return jnp.concatenate(pieces, axis=1)

    def lane_row(col):
        return jnp.broadcast_to(col, (total, LANES)).T

    for copy in small[:4]:
        copy.wait()
    xf = x_ref[...].astype(F32)
    squares = jnp.sum(xf * xf, axis=1, keepdims=True)
    scaled[...] = (xf * row_of(gain_ref)).astype(BF16)
    gate_send[...] = jnp.zeros(gate_send.shape, F32)
    contract = (((1,), (1,)), ((), ()))
    for i, ref in enumerate((ig_ref, fg_ref)):
        gate_send[i * hp : i * hp + heads, :] = lax.dot_general(
            ref[...], scaled[...], contract, preferred_element_type=F32
        )
    gate_send[2 * hp : 3 * hp, :] = lane_row(squares)[0:hp, :]
    pl.semaphore_wait(barrier, (kvn - 1) + len(tp_steps))
    gate_copies = [
        remote(gate_send, gate_recv.at[j - 1], gate_ss.at[j - 1], gate_rs.at[j - 1], "kv", wrap(j))
        for j in range(1, kvn)
    ]
    for copy in gate_copies:
        copy.start()

    def block(buf, c, d, wide):
        if wide == width:
            return buf.at[c, d]
        return buf.at[c, d, :, pl.ds(0, wide)]

    def outer_sends(c, wide):
        found = []
        dests = [d for _, _, d in outside()] + [partner]
        for i, d in enumerate(dests):
            found.append(
                remote(
                    block(part_send, c, d, wide),
                    block(pair_recv, c, d, wide),
                    pair_ss.at[c, i],
                    pair_rs.at[c, d],
                    "kv",
                    partner,
                )
            )
        return found

    def inner_send(c, wide):
        return remote(
            block(part_send, c, partner, wide),
            block(pair_recv, c, partner, wide),
            pair_ss.at[c, 0],
            pair_rs.at[c, partner],
            "kv",
            partner,
        )

    def project(c, wide):
        tile = min(256, wide)

        def body(i, carry):
            cols = pl.ds(pl.multiple_of(i * tile, tile), tile)
            res = jnp.dot(scaled[...], weights[c, :, cols], preferred_element_type=F32)
            part_send[c, :, :, cols] = res.reshape(kvn, rows, tile).astype(BF16)
            return carry

        lax.fori_loop(0, wide // tile, body, 0)

        @pl.when(outer)
        def _():
            for copy in outer_sends(c, wide):
                copy.start()

        @pl.when(leader)
        def _():
            inner_send(c, wide).start()

    def qkv_project(h, carry):
        for copy in qkv_loads(h):
            copy.wait()
        project(h, width)
        return carry

    lax.fori_loop(0, heads, qkv_project, 0)

    def gate_project(c, carry):
        gate_load(c).wait()
        project(heads + c, gate_width)
        return carry

    lax.fori_loop(0, gate_chunks, gate_project, 0)

    wide_out = min(width, local)
    second = []
    for a in range(0, out_hbm.shape[0], local):
        for b in range(0, local, wide_out):
            second.append((out_hbm, a, b, wide_out))
    out_blocks = len(second)
    for b in range(0, hidden_units, width):
        second.append((up_hbm, 0, b, width))
    loads2 = []
    for i, (ref, a, b, wide) in enumerate(second):
        copy = pltpu.make_async_copy(
            ref.at[pl.ds(a, local), pl.ds(b, wide)], weights.at[i, :, pl.ds(0, wide)], w2_sem.at[i]
        )
        copy.start()
        loads2.append(copy)
    down_load = pltpu.make_async_copy(down_hbm, down_w, down_sem.at[0])
    down_load.start()

    for copy in small[4:]:
        copy.wait()
    for h in range(heads):
        norm_h[h] = norm_ref[:, h, :]
        n = dv // LANES
        for i in range(n):
            hg_rows[h, :, i * LANES : (i + 1) * LANES] = head_gain_ref[h * n + i : h * n + i + 1, :].astype(F32)
    max_pad[...] = jnp.zeros(max_pad.shape, F32)
    max_pad[0:heads, 0:rows] = max_ref[...]
    spread = jnp.broadcast_to(bias_ref[...], (heads, heads))
    diag = lax.broadcasted_iota(jnp.int32, (heads, heads), 0) == lax.broadcasted_iota(jnp.int32, (heads, heads), 1)
    bias = jnp.sum(jnp.where(diag, spread, 0.0), axis=1, keepdims=True)
    if heads < hp:
        bias = jnp.concatenate([bias, jnp.zeros((hp - heads, 1), F32)], axis=0)
    for copy in gate_copies:
        copy.wait_recv()
    gsum = gate_send[...]
    for j in range(1, kvn):
        gsum = gsum + gate_recv[j - 1]
    gsum = pltpu.roll(gsum, lax.rem(total - me * rows, total), 1)
    scale = lax.rsqrt(gsum[2 * hp : 3 * hp, :] / model + EPS)
    igate = gsum[0:hp, :] * scale
    z = gsum[hp : 2 * hp, :] * scale + bias
    logf = jnp.minimum(z, 0.0) - jnp.log1p(jnp.exp(-jnp.abs(z)))
    held = logf + max_pad[...]
    new_max = jnp.maximum(held, igate)
    new_max_ref[...] = new_max[0:heads, 0:rows]
    fdec = jnp.exp(held - new_max)
    idec = jnp.exp(igate - new_max)
    floor = jnp.exp(-new_max)
    stacked = jnp.concatenate([fdec, idec, floor, scale, jnp.zeros((LANES - 4 * hp, total), F32)], axis=0).T
    for h in range(heads):
        for i, dst in enumerate((fd_all, id_all, em_all)):
            at = i * hp + h
            dst[h] = jnp.broadcast_to(stacked[0:rows, at : at + 1], (rows, LANES))
    scale_b[...] = jnp.broadcast_to(stacked[0:rows, 3 * hp : 3 * hp + 1], (rows, LANES))

    def cross_sends(c, wide):
        found = []
        for jj, b, d in outside():
            slot = npairs - jj - 1
            found.append(
                (
                    d,
                    remote(
                        block(pair_recv, c, d, wide),
                        block(cross_recv, c, slot, wide),
                        cross_ss.at[c, (jj - 1) * 2 + b],
                        cross_rs.at[c, slot],
                        "kv",
                        d,
                    ),
                )
            )
        return found

    def combine(c, wide):
        for d, copy in cross_sends(c, wide):
            arrived(block(pair_recv, c, d, wide), pair_rs.at[c, d], pair_ss.at[c, 0])
            cols = pl.ds(0, wide)
            both = part_send[c, d, :, cols].astype(F32) + pair_recv[c, d, :, cols].astype(F32)
            pair_recv[c, d, :, cols] = both.astype(BF16)
            copy.start()

    def combine_any(c):
        @pl.when(leader)
        def _():
            if gate_width == width:

                @pl.when(c < chunks)
                def _():
                    combine(c, width)

            else:

                @pl.when(c < heads)
                def _():
                    combine(c, width)

                @pl.when(jnp.logical_and(c >= heads, c < chunks))
                def _():
                    combine(c, gate_width)

    def summed(c, wide):
        arrived(block(pair_recv, c, me, wide), pair_rs.at[c, me], pair_ss.at[c, 0])
        for i in range(npairs - 1):
            arrived(block(cross_recv, c, i, wide), cross_rs.at[c, i], pair_ss.at[c, 0])
        found = []
        for g in range(0, wide, LANES):
            cols = pl.ds(g, LANES)
            val = part_send[c, me, :, cols].astype(F32) + pair_recv[c, me, :, cols].astype(F32)
            for i in range(npairs - 1):
                val = val + cross_recv[c, i, :, cols].astype(F32)
            found.append((val * scale_b[...]).astype(BF16).astype(F32))
        return found

    for c in range(SKEW):
        combine_any(c)

    def head_body(h, carry):
        combine_any(h + SKEW)
        cols = summed(h, width)
        nq = dqk // LANES
        q = jnp.concatenate(cols[:nq], axis=1) * (dqk ** (-0.5))
        k = jnp.concatenate(cols[nq : 2 * nq], axis=1)
        v = jnp.concatenate(cols[2 * nq :], axis=1)
        fd = fd_all[h]
        ik = id_all[h] * k
        nn = fd * norm_h[h] + ik
        norm_h[h] = nn
        denom = jnp.sum(q * nn, axis=1, keepdims=True)
        pad = jnp.zeros((LANES - 2 * rows, dqk), F32)
        turned = jnp.concatenate([ik, q, pad], axis=0).T
        wide_fd = jnp.concatenate([fd] * (dv // LANES), axis=1)
        state_load(h).wait()
        for r in range(rows):
            new = wide_fd[r : r + 1, :] * state[r, h] + turned[:, r : r + 1] * v[r : r + 1, :]
            state[r, h] = new
            numer_s[r : r + 1, :] = jnp.sum(turned[:, rows + r : rows + r + 1] * new, axis=0, keepdims=True)
        readout = numer_s[...] / jnp.maximum(jnp.abs(denom), em_all[h][:, 0:1])
        normed = readout * lax.rsqrt(jnp.sum(readout * readout, axis=1, keepdims=True) / dv + EPS)
        normed_all[h] = normed * hg_rows[h]
        return carry

    lax.fori_loop(0, heads, head_body, 0)

    def own_sends(c):
        src = merged_all.at[c, me]
        return [
            remote(src, src, ag_ss.at[c, j - 1], ag_rs.at[c, me], "kv", wrap(j)) for j in range(1, kvn)
        ]

    def outer_own(c):
        src = merged_all.at[c, me]
        return remote(src, src, ag_ss.at[c, 0], ag_rs.at[c, me], "kv", partner)

    def relay_sends(c):
        src = merged_all.at[c, partner]
        return [
            remote(src, src, relay_ss.at[c, (jj - 1) * 2 + b], ag_rs.at[c, partner], "kv", d)
            for jj, b, d in outside()
        ]

    def relay(c):
        @pl.when(leader)
        def _():
            arrived(merged_all.at[c, partner], ag_rs.at[c, partner], ag_ss.at[c, 0])
            for copy in relay_sends(c):
                copy.start()

    def gate_body(c):
        combine_any(heads + c + SKEW)
        cols = summed(heads + c, gate_width)
        n = dv // LANES
        for i in range(gate_heads):
            o = jnp.concatenate(cols[i * n : (i + 1) * n], axis=1)
            val = jax.nn.sigmoid(o) * normed_all[c * gate_heads + i]
            merged_all[c, me, :, i * dv : (i + 1) * dv] = val.astype(BF16)

        @pl.when(leader)
        def _():
            for copy in own_sends(c):
                copy.start()

        @pl.when(outer)
        def _():
            outer_own(c).start()

    def out_project(c):
        @pl.when(outer)
        def _():
            arrived(merged_all.at[c, partner], ag_rs.at[c, partner], ag_ss.at[c, 0])

        for _, _, d in outside():
            arrived(merged_all.at[c, d], ag_rs.at[c, d], ag_ss.at[c, 0])
        tile = min(256, wide_out)
        lhs = merged_all[c].reshape(total, gate_width)
        for i, (ref, a, b, wide) in enumerate(second[:out_blocks]):
            if not a <= c * gate_width < a + local:
                continue
            if c * gate_width == a:
                loads2[i].wait()

            def body(t, carry, i=i, a=a, b=b):
                cols = pl.ds(pl.multiple_of(t * tile, tile), tile)
                into = pl.ds(pl.multiple_of(b + t * tile, tile), tile)
                w = weights[i, c * gate_width - a : (c + 1) * gate_width - a, cols]
                res = jnp.dot(lhs, w, preferred_element_type=F32)
                if c == 0:
                    part[:, into] = res
                else:
                    part[:, into] += res
                return carry

            lax.fori_loop(0, wide // tile, body, 0)

    for c in range(gate_chunks):
        gate_body(c)
        if c >= 1:
            relay(c - 1)
        if c >= 2:
            out_project(c - 2)
    relay(gate_chunks - 1)
    for c in range(max(gate_chunks - 2, 0), gate_chunks):
        out_project(c)

    half = total // 2
    piece = local // PIECES
    low = tme % 2
    mate = tme + 1 - 2 * low
    mine = pl.ds(pl.multiple_of(low * half, half), half)
    theirs = pl.ds(pl.multiple_of((1 - low) * half, half), half)

    def tp_sum(n, base):
        sent = []
        stage = []
        for p in range(PIECES):
            cols = slice(p * piece, (p + 1) * piece)
            half_send[n, p] = part[theirs, cols].astype(BF16)
            copy = remote(half_send.at[n, p], half_recv.at[n, p], half_ss.at[n, p], half_rs.at[n, p], "tp", mate)
            copy.start()
            stage.append(copy)
        sent += stage
        for p in range(PIECES):
            cols = slice(p * piece, (p + 1) * piece)
            stage[p].wait_recv()
            val = part[mine, cols] + half_recv[n, p].astype(F32)
            if len(tp_steps) > 1:
                y_send[n, 0, p] = val.astype(BF16)
            else:
                full[n, low, p] = (base(p) + val).astype(BF16)
        for i, s in enumerate(tp_steps[1:]):
            stage = []
            for p in range(PIECES):
                copy = remote(
                    y_send.at[n, i, p], y_recv.at[n, i, p], y_ss.at[n, i, p], y_rs.at[n, i, p], "tp", tp_peer(s)
                )
                copy.start()
                stage.append(copy)
            sent += stage
            for p in range(PIECES):
                stage[p].wait_recv()
                val = y_send[n, i, p].astype(F32) + y_recv[n, i, p].astype(F32)
                if i + 2 < len(tp_steps):
                    y_send[n, i + 1, p] = val.astype(BF16)
                else:
                    full[n, low, p] = (base(p) + val).astype(BF16)
        stage = []
        for p in range(PIECES):
            src = full.at[n, low, p]
            copy = remote(src, src, full_ss.at[n, p], full_rs.at[n, p], "tp", mate)
            copy.start()
            stage.append(copy)
        for copy in stage:
            copy.wait_recv()
        return sent + stage

    sent = tp_sum(0, lambda p: x_ref[mine, p * piece : (p + 1) * piece].astype(F32))
    mix_row = row_of(mix_gain_ref)
    sq = jnp.zeros((total, 1), F32)
    for p in range(PIECES):
        cols = slice(p * piece, (p + 1) * piece)
        rf = jnp.concatenate([full[0, 0, p], full[0, 1, p]], axis=0).astype(F32)
        sq = sq + jnp.sum(rf * rf, axis=1, keepdims=True)
        scaled[:, cols] = (rf * mix_row[:, cols]).astype(BF16)
    sq_send[...] = lane_row(sq)[0:8, :]
    sq_copies = [
        remote(sq_send, sq_recv.at[j - 1], sq_ss.at[j - 1], sq_rs.at[j - 1], "kv", wrap(j)) for j in range(1, kvn)
    ]
    for copy in sq_copies:
        copy.start()

    for copy in loads2[out_blocks:]:
        copy.wait()
    per_slot = width // up_width

    def outer_up(c):
        return remote(upb.at[0, c], upb.at[1, c], up_ss.at[c], up_rs.at[c], "kv", partner)

    def up_body(c, carry):
        slot = out_blocks + c // per_slot
        cols = pl.ds(pl.multiple_of((c % per_slot) * up_width, up_width), up_width)
        upb[0, c] = jnp.dot(scaled[...], weights[slot, :, cols], preferred_element_type=F32).astype(BF16)

        @pl.when(outer)
        def _():
            outer_up(c).start()

        return carry

    lax.fori_loop(0, up_chunks, up_body, 0)
    for copy in sq_copies:
        copy.wait_recv()
    sq_sum = sq_send[...]
    for j in range(1, kvn):
        sq_sum = sq_sum + sq_recv[j - 1]
    two = lax.rsqrt(sq_sum[0:1, :] / model + EPS)
    scale_two[...] = jnp.broadcast_to(two, (LANES, total)).T

    def up_cross_sends(c):
        found = []
        for jj in range(1, npairs):
            other = lax.rem(pair + jj, npairs)
            head = 2 * other + 1 - (2 * other) // npairs
            slot = npairs - jj - 1
            found.append(
                remote(upb.at[1, c], up_cross.at[c, slot], upx_ss.at[c, jj - 1], upx_rs.at[c, slot], "kv", head)
            )
        return found

    def hidden_send(c):
        return remote(upb.at[0, c], upb.at[1, c], hid_ss.at[c], hid_rs.at[c], "kv", partner)

    def up_combine(c):
        arrived(upb.at[1, c], up_rs.at[c], up_ss.at[c])
        both = upb[0, c].astype(F32) + upb[1, c].astype(F32)
        upb[1, c] = both.astype(BF16)
        for copy in up_cross_sends(c):
            copy.start()

    def up_finish(c):
        for i in range(npairs - 1):
            arrived(up_cross.at[c, i], upx_rs.at[c, i], up_ss.at[c])
        for g in range(0, up_width, LANES):
            cols = pl.ds(g, LANES)
            val = upb[1, c, :, cols].astype(F32)
            for i in range(npairs - 1):
                val = val + up_cross[c, i, :, cols].astype(F32)
            act = jnp.maximum(val * scale_two[...], 0.0)
            upb[0, c, :, cols] = (act * act).astype(BF16)
        hidden_send(c).start()

    down_load.wait()
    down_tile = min(256, local)
    part[...] = jnp.zeros(part.shape, F32)

    def down_project(c, which):
        rws = pl.ds(pl.multiple_of(c * up_width, up_width), up_width)

        def body(t, carry):
            cols = pl.ds(pl.multiple_of(t * down_tile, down_tile), down_tile)
            part[:, cols] += jnp.dot(upb[which, c], down_w[rws, cols], preferred_element_type=F32)
            return carry

        lax.fori_loop(0, local // down_tile, body, 0)

    @pl.when(leader)
    def _():
        def tick(c, carry):
            @pl.when(c < up_chunks)
            def _():
                up_combine(c)

            @pl.when(c >= UP_SKEW)
            def _():
                up_finish(c - UP_SKEW)
                down_project(c - UP_SKEW, 0)

            return carry

        lax.fori_loop(0, up_chunks + UP_SKEW, tick, 0)

    @pl.when(outer)
    def _():
        def tick(c, carry):
            arrived(upb.at[1, c], hid_rs.at[c], up_ss.at[c])
            down_project(c, 1)
            return carry

        lax.fori_loop(0, up_chunks, tick, 0)

    def resid(p):
        return full[0, low, p].astype(F32)

    sent += tp_sum(1, resid)
    for p in range(PIECES):
        cols = slice(p * piece, (p + 1) * piece)
        for b in range(2):
            mixed_ref[b * half : (b + 1) * half, cols] = full[1, b, p]
    for h in range(heads):
        new_norm_ref[:, h, :] = norm_h[h]

    for copy in sent + gate_copies + sq_copies:
        copy.wait_send()

    def drain(c, wide):
        @pl.when(outer)
        def _():
            for copy in outer_sends(c, wide):
                copy.wait_send()

        @pl.when(leader)
        def _():
            inner_send(c, wide).wait_send()
            for _, copy in cross_sends(c, wide):
                copy.wait_send()

    def drain_qkv(c, carry):
        drain(c, width)
        return carry

    def drain_gate(c, carry):
        drain(heads + c, gate_width)

        @pl.when(outer)
        def _():
            outer_own(c).wait_send()

        @pl.when(leader)
        def _():
            for copy in own_sends(c) + relay_sends(c):
                copy.wait_send()

        return carry

    def drain_up(c, carry):
        @pl.when(outer)
        def _():
            outer_up(c).wait_send()

        @pl.when(leader)
        def _():
            for copy in up_cross_sends(c) + [hidden_send(c)]:
                copy.wait_send()

        return carry

    lax.fori_loop(0, heads, drain_qkv, 0)
    lax.fori_loop(0, gate_chunks, drain_gate, 0)
    lax.fori_loop(0, up_chunks, drain_up, 0)


def flush(*refs):
    sem = refs[-1]
    n = (len(refs) - 1) // 2
    copies = []
    for i in range(1, n):
        copies.append((refs[i], refs[n + i]))
    for r in range(refs[0].shape[0]):
        copies.append((refs[0].at[r], refs[n].at[r]))
    started = []
    for i, (src, dst) in enumerate(copies):
        copy = pltpu.make_async_copy(src, dst, sem.at[i])
        copy.start()
        started.append(copy)
    for copy in started:
        copy.wait()


def per_device(
    kvn,
    tpn,
    x_rows,
    in_gain,
    query_weight,
    key_weight,
    value_weight,
    outgate_weight,
    input_gate_weight,
    forget_gate_weight,
    forget_bias,
    state_matrix,
    state_norm,
    state_max,
    head_gain,
    out_weight,
    mix_gain,
    up_weight,
    down_weight,
):
    total, local = x_rows.shape
    rows, heads, dqk, dv = state_matrix.shape
    hidden_units = up_weight.shape[1]
    width = 2 * dqk + dv
    gate_heads = min(2, heads)
    gate_width = gate_heads * dv
    gate_chunks = heads // gate_heads
    chunks = heads + gate_chunks
    up_width = min(256, width)
    up_chunks = hidden_units // up_width
    wide_out = min(width, local)
    slots2 = (heads * dv // local) * (local // wide_out) + hidden_units // width
    slots = max(chunks, slots2)
    hp = -(-heads // 8) * 8
    npairs = kvn // 2
    np1 = max(npairs - 1, 1)
    steps = max((tpn - 1).bit_length() - 1, 1)
    half, piece = total // 2, local // PIECES
    vmem = pl.BlockSpec(memory_space=pltpu.VMEM)
    hbm = pl.BlockSpec(memory_space=pl.ANY)
    V = pltpu.VMEM
    dma = pltpu.SemaphoreType.DMA
    k1 = kvn - 1
    gains = (local // LANES, LANES)
    hg_shape = (heads * dv // LANES, LANES)
    scratch = [
        V((total, local), BF16),
        V(gains, BF16),
        V((heads, local), BF16),
        V((heads, local), BF16),
        V((1, heads), F32),
        V((rows, heads, dqk), F32),
        V((heads, rows), F32),
        V(hg_shape, BF16),
        V(gains, BF16),
        V((slots, local, width), BF16),
        V((hidden_units, local), BF16),
        V((total, local), BF16),
        V((total, local), F32),
        V((3 * hp, total), F32),
        V((k1, 3 * hp, total), F32),
        V((hp, total), F32),
        V((chunks, kvn, rows, width), BF16),
        V((chunks, kvn, rows, width), BF16),
        V((chunks, np1, rows, width), BF16),
        V((heads, rows, dqk), F32),
        V((heads, rows, LANES), F32),
        V((heads, rows, LANES), F32),
        V((heads, rows, LANES), F32),
        V((rows, LANES), F32),
        V((heads, 1, dv), F32),
        V((rows, dv), F32),
        V((heads, rows, dv), F32),
        V((gate_chunks, kvn, rows, gate_width), BF16),
        V((2, PIECES, half, piece), BF16),
        V((2, PIECES, half, piece), BF16),
        V((2, steps, PIECES, half, piece), BF16),
        V((2, steps, PIECES, half, piece), BF16),
        V((2, 2, PIECES, half, piece), BF16),
        V((8, total), F32),
        V((k1, 8, total), F32),
        V((total, LANES), F32),
        V((2, up_chunks, total, up_width), BF16),
        V((up_chunks, np1, total, up_width), BF16),
        dma((9,)),
        dma((chunks, 3)),
        dma((slots2,)),
        dma((1,)),
        dma((heads,)),
        dma((k1,)),
        dma((k1,)),
        dma((chunks, k1)),
        dma((chunks, kvn)),
        dma((chunks, 2 * np1)),
        dma((chunks, np1)),
        dma((gate_chunks, k1)),
        dma((gate_chunks, 2 * np1)),
        dma((gate_chunks, kvn)),
        dma((2, PIECES)),
        dma((2, PIECES)),
        dma((2, steps, PIECES)),
        dma((2, steps, PIECES)),
        dma((2, PIECES)),
        dma((2, PIECES)),
        dma((k1,)),
        dma((k1,)),
        dma((up_chunks,)),
        dma((up_chunks,)),
        dma((up_chunks, np1)),
        dma((up_chunks, np1)),
        dma((up_chunks,)),
        dma((up_chunks,)),
    ]
    state_bytes = state_matrix.size * 4
    outs = pl.pallas_call(
        functools.partial(kernel, kvn, tpn, width, gate_heads, up_width),
        out_shape=(
            pltpu.VMEM((total, local), BF16),
            pltpu.VMEM(state_matrix.shape, F32),
            pltpu.VMEM(state_norm.shape, F32),
            pltpu.VMEM((heads, rows), F32),
        ),
        in_specs=[hbm] * 17,
        out_specs=(vmem,) * 4,
        scratch_shapes=scratch,
        compiler_params=pltpu.CompilerParams(
            collective_id=0,
            has_side_effects=True,
            vmem_limit_bytes=67043328 - state_bytes - (1 << 19),
        ),
    )(
        x_rows,
        in_gain.reshape(gains),
        query_weight,
        key_weight,
        value_weight,
        outgate_weight,
        input_gate_weight.T,
        forget_gate_weight.T,
        forget_bias.reshape(1, heads),
        state_matrix,
        state_norm,
        state_max.T,
        head_gain.reshape(hg_shape),
        out_weight,
        mix_gain.reshape(gains),
        up_weight,
        down_weight,
    )
    mixed, new_matrix, new_norm, new_max = outs
    new_matrix, mixed, new_norm, new_max = pl.pallas_call(
        flush,
        out_shape=(
            jax.ShapeDtypeStruct(state_matrix.shape, F32),
            jax.ShapeDtypeStruct((total, local), BF16),
            jax.ShapeDtypeStruct(state_norm.shape, F32),
            jax.ShapeDtypeStruct((heads, rows), F32),
        ),
        in_specs=[hbm] * 4,
        out_specs=(hbm,) * 4,
        scratch_shapes=[dma((rows + 3,))],
        compiler_params=pltpu.CompilerParams(vmem_limit_bytes=1 << 20),
    )(new_matrix, mixed, new_norm, new_max)
    return (mixed, new_matrix, new_norm, new_max.T)


def solution(mesh):
    placed = (
        P("grp", "kv"),
        P("kv"),
        P("kv", "tp"),
        P("kv", "tp"),
        P("kv", "tp"),
        P("kv", "tp"),
        P("kv", "tp"),
        P("kv", "tp"),
        P("tp"),
        P(("grp", "kv"), "tp", None, None),
        P(("grp", "kv"), "tp", None),
        P(("grp", "kv"), "tp"),
        P("tp"),
        P("tp", "kv"),
        P("kv"),
        P("kv", "tp"),
        P("tp", "kv"),
    )
    return jax.shard_map(
        functools.partial(per_device, mesh.shape["kv"], mesh.shape["tp"]),
        mesh=mesh,
        in_specs=placed,
        out_specs=(
            P("grp", "kv"),
            P(("grp", "kv"), "tp", None, None),
            P(("grp", "kv"), "tp", None),
            P(("grp", "kv"), "tp"),
        ),
        check_vma=False,
    )
```

time: 181 us -> 136 us (0.75)
  Pallas kernels: 145 us -> 112 us
  local copies, waits for them, and re-layouts: 33.7 us -> 23.9 us
    pallas_call x1 -> x2, Pallas kernels: 145 us -> 112 us  [the longest x1 100 us: per_device(): pl.pallas_call(functools.partial(kernel, kvn, tpn, width, gate_heads, up_...]
    unnamed x9 -> x8, local copies, waits for them, and re-layouts: 29.9 us -> 23.9 us
    reshape x3 -> x0, local copies, waits for them, and re-layouts: 3.83 us -> none  [the longest x1 1.29 us: per_device(): head_gain.astype(F32).reshape(heads, dv)]
where the time goes in v1:
time: 136 us
  Pallas kernels  112 us (82%)
  local copies, waits for them, and re-layouts  23.9 us (18%)
    pallas_call x1, Pallas kernels, per_device(): pl.pallas_call(functools.partial(kernel, kvn, tpn, width, gate_heads, up_...  100 us
    unnamed x8, local copies, waits for them, and re-layouts  23.9 us
    pallas_call x1, Pallas kernels, per_device(): pl.pallas_call(flush, out_shape=(jax.ShapeDtypeStruct(state_matrix.shape,...  11.3 us

profile of v1, /device:TPU:0, one launch (start us, length us, event | category | flops | bytes accessed | tf_op | source)
XLA Modules:
  0.0 136.3 jit_solution(2167766728337872584)
XLA Ops:
  0.6 100.5 %shard_map.192 = (bf16[128,1024]{1,0:T(8,128)(2,1)S(1)}, f32[32,8,128,256]{3,2,1,0:T(8,128)S(1)}, f32[32,8,128]{2,1,0:T(8,128)S(1)}, f32[8,32]{1,0:T(8,128)S(1)}) custom-call(bf16[128,1024]{1,0:T(8,128)(2,1)} %x_hbm.1, bf16[8,128]{1,0:T(8,128)(2,1)} %bitcast.12, bf16[1024,1024]{1,0:T(8,128)(2,1)} %q_hbm.1, bf16[1024,1024]{1,0:T(8,128)(2,1)} %k_hbm.1, ...), custom_call_target="tpu_custom_call" | custom-call | tf_op jit(solution)/shard_map/pallas_call | solution.py:888
  101.1 0.0 copy-start
  101.1 11.7 %copy-done = f32[32,8,128,256]{3,2,1,0:T(8,128)} copy-done((f32[32,8,128,256]{3,2,1,0:T(8,128)}, f32[32,8,128,256]{3,2,1,0:T(8,128)S(1)}, u32[]{:S(2)}) %copy-start) | copy-done | bytes 33554456
  112.8 0.0 copy-start.2
  112.8 0.7 copy-done.2
  113.5 0.0 copy-start.1
  113.5 10.5 %copy-done.1 = f32[32,8,128,256]{3,2,1,0:T(8,128)S(1)} copy-done((f32[32,8,128,256]{3,2,1,0:T(8,128)S(1)}, f32[32,8,128,256]{3,2,1,0:T(8,128)}, u32[]{:S(2)}) %copy-start.1) | copy-done | bytes 33554456
  124.0 0.0 copy-start.3
  124.0 0.9 copy-done.3
  125.0 11.3 %shard_map.193 = (f32[32,8,128,256]{3,2,1,0:T(8,128)}, bf16[128,1024]{1,0:T(8,128)(2,1)}, f32[32,8,128]{2,1,0:T(8,128)}, f32[8,32]{1,0:T(8,128)}) custom-call(f32[32,8,128,256]{3,2,1,0:T(8,128)S(1)} %copy-done.1, bf16[128,1024]{1,0:T(8,128)(2,1)S(1)} %copy-done.3, f32[32,8,128]{2,1,0:T(8,128)S(1)} %get-tuple-element.14.refs_2_, ...), custom_call_target="tpu_custom_call" | custom-call | tf_op jit(solution)/shard_map/pallas_call | solution.py:924
Async XLA Ops:
  101.1 11.7 %copy-start = (f32[32,8,128,256]{3,2,1,0:T(8,128)}, f32[32,8,128,256]{3,2,1,0:T(8,128)S(1)}, u32[]{:S(2)}) copy-start(f32[32,8,128,256]{3,2,1,0:T(8,128)S(1)} %get-tuple-element.12.refs_0_) | copy-start | bytes 100663296
  112.8 0.7 copy-start.2
  113.5 10.5 %copy-start.1 = (f32[32,8,128,256]{3,2,1,0:T(8,128)S(1)}, f32[32,8,128,256]{3,2,1,0:T(8,128)}, u32[]{:S(2)}) copy-start(f32[32,8,128,256]{3,2,1,0:T(8,128)} %copy-done) | copy-start | bytes 100663296
  124.0 0.9 copy-start.3

commit v2 on v1

--- a/solution.py
+++ b/solution.py
@@ -14,7 +14,8 @@
 BF16 = jnp.bfloat16
 PIECES = 2
 SKEW = 2
-UP_SKEW = 3
+UP_SKEW = 2
+AHEAD = 5
 
 
 def kernel(
@@ -70,7 +71,7 @@
     scale_b,
     hg_rows,
     numer_s,
-    normed_all,
+    opened,
     merged_all,
     half_send,
     half_recv,
@@ -166,34 +167,28 @@
             (mix_gain_hbm, mix_gain_ref),
         )
     ):
-        copy = pltpu.make_async_copy(src, dst, small_sem.at[i])
+        small.append(pltpu.make_async_copy(src, dst, small_sem.at[i]))
+    for copy in small[:4]:
         copy.start()
-        small.append(copy)
 
     def qkv_loads(h):
         found = []
         at = 0
         for i, (ref, extent) in enumerate(((q_hbm, dqk), (k_hbm, dqk), (v_hbm, dv))):
             src = ref.at[:, pl.ds(pl.multiple_of(h * extent, extent), extent)]
-            found.append(pltpu.make_async_copy(src, weights.at[h, :, pl.ds(at, extent)], w_sem.at[h, i]))
+            found.append(pltpu.make_async_copy(src, weights.at[gate_chunks + h, :, pl.ds(at, extent)], w_sem.at[gate_chunks + h, i]))
             at += extent
         return found
 
     def gate_load(c):
         src = o_hbm.at[:, pl.ds(pl.multiple_of(c * gate_width, gate_width), gate_width)]
-        return pltpu.make_async_copy(src, weights.at[heads + c, :, pl.ds(0, gate_width)], w_sem.at[heads + c, 0])
-
-    for h in range(heads):
-        for copy in qkv_loads(h):
-            copy.start()
-    for c in range(gate_chunks):
+        return pltpu.make_async_copy(src, weights.at[c, :, pl.ds(0, gate_width)], w_sem.at[c, 0])
+
+    for c in range(min(1, gate_chunks)):
         gate_load(c).start()
 
     def state_load(h):
         return pltpu.make_async_copy(state_hbm.at[:, h], state.at[:, h], state_sem.at[h])
-
-    for h in range(heads):
-        state_load(h).start()
 
     tp_steps = []
     s = 1
@@ -219,6 +214,13 @@
 
     for copy in small[:4]:
         copy.wait()
+    for c in range(1, gate_chunks):
+        gate_load(c).start()
+    for h in range(heads):
+        for copy in qkv_loads(h):
+            copy.start()
+    for copy in small[4:]:
+        copy.start()
     xf = x_ref[...].astype(F32)
     squares = jnp.sum(xf * xf, axis=1, keepdims=True)
     scaled[...] = (xf * row_of(gain_ref)).astype(BF16)
@@ -269,7 +271,7 @@
         )
 
     def project(c, wide):
-        tile = min(256, wide)
+        tile = min(512, wide)
 
         def body(i, carry):
             cols = pl.ds(pl.multiple_of(i * tile, tile), tile)
@@ -279,7 +281,7 @@
 
         lax.fori_loop(0, wide // tile, body, 0)
 
-        @pl.when(outer)
+        @pl.when(jnp.logical_and(outer, c < AHEAD))
         def _():
             for copy in outer_sends(c, wide):
                 copy.start()
@@ -287,21 +289,22 @@
         @pl.when(leader)
         def _():
             inner_send(c, wide).start()
+
+    def gate_project(c, carry):
+        gate_load(c).wait()
+        project(c, gate_width)
+        return carry
+
+    lax.fori_loop(0, gate_chunks, gate_project, 0)
 
     def qkv_project(h, carry):
         for copy in qkv_loads(h):
             copy.wait()
-        project(h, width)
+        state_load(h).start()
+        project(gate_chunks + h, width)
         return carry
 
     lax.fori_loop(0, heads, qkv_project, 0)
-
-    def gate_project(c, carry):
-        gate_load(c).wait()
-        project(heads + c, gate_width)
-        return carry
-
-    lax.fori_loop(0, gate_chunks, gate_project, 0)
 
     wide_out = min(width, local)
     second = []
@@ -396,13 +399,35 @@
 
             else:
 
-                @pl.when(c < heads)
+                @pl.when(c < gate_chunks)
+                def _():
+                    combine(c, gate_width)
+
+                @pl.when(jnp.logical_and(c >= gate_chunks, c < chunks))
                 def _():
                     combine(c, width)
 
-                @pl.when(jnp.logical_and(c >= heads, c < chunks))
+    def send_ahead(c):
+        @pl.when(outer)
+        def _():
+            if gate_width == width:
+
+                @pl.when(c < chunks)
                 def _():
-                    combine(c, gate_width)
+                    for copy in outer_sends(c, width):
+                        copy.start()
+
+            else:
+
+                @pl.when(c < gate_chunks)
+                def _():
+                    for copy in outer_sends(c, gate_width):
+                        copy.start()
+
+                @pl.when(jnp.logical_and(c >= gate_chunks, c < chunks))
+                def _():
+                    for copy in outer_sends(c, width):
+                        copy.start()
 
     def summed(c, wide):
         arrived(block(pair_recv, c, me, wide), pair_rs.at[c, me], pair_ss.at[c, 0])
@@ -417,12 +442,92 @@
             found.append((val * scale_b[...]).astype(BF16).astype(F32))
         return found
 
+    last = heads - 1
+
+    def own_sends(h):
+        src = merged_all.at[h, me]
+        return [
+            remote(src, src, ag_ss.at[h, j - 1], ag_rs.at[h, me], "kv", wrap(j)) for j in range(1, kvn)
+        ]
+
+    def outer_own(h):
+        src = merged_all.at[h, me]
+        return remote(src, src, ag_ss.at[h, 0], ag_rs.at[h, me], "kv", partner)
+
+    def relay_sends(h):
+        src = merged_all.at[h, partner]
+        return [
+            remote(src, src, relay_ss.at[h, (jj - 1) * 2 + b], ag_rs.at[h, partner], "kv", d)
+            for jj, b, d in outside()
+        ]
+
+    def relay(h):
+        @pl.when(leader)
+        def _():
+            arrived(merged_all.at[h, partner], ag_rs.at[h, partner], ag_ss.at[h, 0])
+            for copy in relay_sends(h):
+                copy.start()
+
+    def spread_merged(h):
+        direct = jnp.logical_or(leader, h == last)
+
+        @pl.when(direct)
+        def _():
+            for copy in own_sends(h):
+                copy.start()
+
+        @pl.when(jnp.logical_not(direct))
+        def _():
+            outer_own(h).start()
+
+    out_tile = min(256, wide_out)
+    out_cols = local // wide_out
+
+    def out_project(batch, first):
+        for h in batch:
+            for _, _, d in outside():
+                arrived(merged_all.at[h, d], ag_rs.at[h, d], ag_ss.at[h, 0])
+
+            @pl.when(jnp.logical_or(outer, h == last))
+            def _(h=h):
+                arrived(merged_all.at[h, partner], ag_rs.at[h, partner], ag_ss.at[h, 0])
+
+        for b in range(out_cols):
+
+            def body(t, carry, b=b):
+                cols = pl.ds(pl.multiple_of(t * out_tile, out_tile), out_tile)
+                into = pl.ds(pl.multiple_of(b * wide_out + t * out_tile, out_tile), out_tile)
+                acc = jnp.zeros((total, out_tile), F32)
+                for h in batch:
+                    slot = (h * dv // local) * out_cols + b
+                    at = (h * dv) % local
+                    lhs = merged_all[h].reshape(total, dv)
+                    acc = acc + jnp.dot(lhs, weights[slot, at : at + dv, cols], preferred_element_type=F32)
+                if first:
+                    part[:, into] = acc
+                else:
+                    part[:, into] += acc
+                return carry
+
+            lax.fori_loop(0, wide_out // out_tile, body, 0)
+
     for c in range(SKEW):
         combine_any(c)
 
+    def gate_body(c, carry):
+        combine_any(c + SKEW)
+        cols = summed(c, gate_width)
+        n = dv // LANES
+        for i in range(gate_heads):
+            o = jnp.concatenate(cols[i * n : (i + 1) * n], axis=1)
+            opened[c * gate_heads + i] = jax.nn.sigmoid(o)
+        send_ahead(c + AHEAD)
+        return carry
+
+    lax.fori_loop(0, gate_chunks, gate_body, 0)
     def head_body(h, carry):
-        combine_any(h + SKEW)
-        cols = summed(h, width)
+        combine_any(gate_chunks + h + SKEW)
+        cols = summed(gate_chunks + h, width)
         nq = dqk // LANES
         q = jnp.concatenate(cols[:nq], axis=1) * (dqk ** (-0.5))
         k = jnp.concatenate(cols[nq : 2 * nq], axis=1)
@@ -442,90 +547,26 @@
             numer_s[r : r + 1, :] = jnp.sum(turned[:, rows + r : rows + r + 1] * new, axis=0, keepdims=True)
         readout = numer_s[...] / jnp.maximum(jnp.abs(denom), em_all[h][:, 0:1])
         normed = readout * lax.rsqrt(jnp.sum(readout * readout, axis=1, keepdims=True) / dv + EPS)
-        normed_all[h] = normed * hg_rows[h]
+        merged_all[h, me] = (opened[h] * (normed * hg_rows[h])).astype(BF16)
+        spread_merged(h)
+
+        send_ahead(gate_chunks + h + AHEAD)
+        for early in range(last):
+            when = min(early + 3, (early + heads + 1) // 2, last)
+
+            @pl.when(h == when)
+            def _(early=early):
+                relay(early)
+
         return carry
 
     lax.fori_loop(0, heads, head_body, 0)
-
-    def own_sends(c):
-        src = merged_all.at[c, me]
-        return [
-            remote(src, src, ag_ss.at[c, j - 1], ag_rs.at[c, me], "kv", wrap(j)) for j in range(1, kvn)
-        ]
-
-    def outer_own(c):
-        src = merged_all.at[c, me]
-        return remote(src, src, ag_ss.at[c, 0], ag_rs.at[c, me], "kv", partner)
-
-    def relay_sends(c):
-        src = merged_all.at[c, partner]
-        return [
-            remote(src, src, relay_ss.at[c, (jj - 1) * 2 + b], ag_rs.at[c, partner], "kv", d)
-            for jj, b, d in outside()
-        ]
-
-    def relay(c):
-        @pl.when(leader)
-        def _():
-            arrived(merged_all.at[c, partner], ag_rs.at[c, partner], ag_ss.at[c, 0])
-            for copy in relay_sends(c):
-                copy.start()
-
-    def gate_body(c):
-        combine_any(heads + c + SKEW)
-        cols = summed(heads + c, gate_width)
-        n = dv // LANES
-        for i in range(gate_heads):
-            o = jnp.concatenate(cols[i * n : (i + 1) * n], axis=1)
-            val = jax.nn.sigmoid(o) * normed_all[c * gate_heads + i]
-            merged_all[c, me, :, i * dv : (i + 1) * dv] = val.astype(BF16)
-
-        @pl.when(leader)
-        def _():
-            for copy in own_sends(c):
-                copy.start()
-
-        @pl.when(outer)
-        def _():
-            outer_own(c).start()
-
-    def out_project(c):
-        @pl.when(outer)
-        def _():
-            arrived(merged_all.at[c, partner], ag_rs.at[c, partner], ag_ss.at[c, 0])
-
-        for _, _, d in outside():
-            arrived(merged_all.at[c, d], ag_rs.at[c, d], ag_ss.at[c, 0])
-        tile = min(256, wide_out)
-        lhs = merged_all[c].reshape(total, gate_width)
-        for i, (ref, a, b, wide) in enumerate(second[:out_blocks]):
-            if not a <= c * gate_width < a + local:
-                continue
-            if c * gate_width == a:
-                loads2[i].wait()
-
-            def body(t, carry, i=i, a=a, b=b):
-                cols = pl.ds(pl.multiple_of(t * tile, tile), tile)
-                into = pl.ds(pl.multiple_of(b + t * tile, tile), tile)
-                w = weights[i, c * gate_width - a : (c + 1) * gate_width - a, cols]
-                res = jnp.dot(lhs, w, preferred_element_type=F32)
-                if c == 0:
-                    part[:, into] = res
-                else:
-                    part[:, into] += res
-                return carry
-
-            lax.fori_loop(0, wide // tile, body, 0)
-
-    for c in range(gate_chunks):
-        gate_body(c)
-        if c >= 1:
-            relay(c - 1)
-        if c >= 2:
-            out_project(c - 2)
-    relay(gate_chunks - 1)
-    for c in range(max(gate_chunks - 2, 0), gate_chunks):
-        out_project(c)
+    for copy in loads2[:out_blocks]:
+        copy.wait()
+    late = max(heads - 2, 0)
+    if late:
+        out_project(range(late), True)
+    out_project(range(late, heads), late == 0)
 
     half = total // 2
     piece = local // PIECES
@@ -718,20 +759,26 @@
             for _, copy in cross_sends(c, wide):
                 copy.wait_send()
 
-    def drain_qkv(c, carry):
-        drain(c, width)
+    def drain_gate(c, carry):
+        drain(c, gate_width)
         return carry
 
-    def drain_gate(c, carry):
-        drain(heads + c, gate_width)
-
-        @pl.when(outer)
-        def _():
-            outer_own(c).wait_send()
-
-        @pl.when(leader)
-        def _():
-            for copy in own_sends(c) + relay_sends(c):
+    def drain_qkv(h, carry):
+        drain(gate_chunks + h, width)
+        direct = jnp.logical_or(leader, h == last)
+
+        @pl.when(direct)
+        def _():
+            for copy in own_sends(h):
+                copy.wait_send()
+
+        @pl.when(jnp.logical_not(direct))
+        def _():
+            outer_own(h).wait_send()
+
+        @pl.when(jnp.logical_and(leader, h < last))
+        def _():
+            for copy in relay_sends(h):
                 copy.wait_send()
 
         return carry
@@ -844,7 +891,7 @@
         V((heads, 1, dv), F32),
         V((rows, dv), F32),
         V((heads, rows, dv), F32),
-        V((gate_chunks, kvn, rows, gate_width), BF16),
+        V((heads, kvn, rows, dv), BF16),
         V((2, PIECES, half, piece), BF16),
         V((2, PIECES, half, piece), BF16),
         V((2, steps, PIECES, half, piece), BF16),
@@ -866,9 +913,9 @@
         dma((chunks, kvn)),
         dma((chunks, 2 * np1)),
         dma((chunks, np1)),
-        dma((gate_chunks, k1)),
-        dma((gate_chunks, 2 * np1)),
-        dma((gate_chunks, kvn)),
+        dma((heads, k1)),
+        dma((heads, 2 * np1)),
+        dma((heads, kvn)),
         dma((2, PIECES)),
         dma((2, PIECES)),
         dma((2, steps, PIECES)),
@@ -921,19 +968,14 @@
         down_weight,
     )
     mixed, new_matrix, new_norm, new_max = outs
-    new_matrix, mixed, new_norm, new_max = pl.pallas_call(
+    new_matrix, mixed = pl.pallas_call(
         flush,
-        out_shape=(
-            jax.ShapeDtypeStruct(state_matrix.shape, F32),
-            jax.ShapeDtypeStruct((total, local), BF16),
-            jax.ShapeDtypeStruct(state_norm.shape, F32),
-            jax.ShapeDtypeStruct((heads, rows), F32),
-        ),
-        in_specs=[hbm] * 4,
-        out_specs=(hbm,) * 4,
+        out_shape=(jax.ShapeDtypeStruct(state_matrix.shape, F32), jax.ShapeDtypeStruct((total, local), BF16)),
+        in_specs=[hbm] * 2,
+        out_specs=(hbm,) * 2,
         scratch_shapes=[dma((rows + 3,))],
         compiler_params=pltpu.CompilerParams(vmem_limit_bytes=1 << 20),
-    )(new_matrix, mixed, new_norm, new_max)
+    )(new_matrix, mixed)
     return (mixed, new_matrix, new_norm, new_max.T)
 
 

time: 136 us -> 108 us (0.79)
  local copies, waits for them, and re-layouts: 23.9 us -> 1.25 us
  Pallas kernels: 112 us -> 106 us
    unnamed x8 -> x2, local copies, waits for them, and re-layouts: 23.9 us -> 1.25 us
    pallas_call x1, Pallas kernels: 100 us -> 94.9 us  [per_device(): pl.pallas_call(functools.partial(kernel, kvn, tpn, width, gate_heads, up_...]
where the time goes in v2:
time: 108 us
  Pallas kernels  106 us (98%)
  local copies, waits for them, and re-layouts  1.25 us (1%)
    pallas_call x1, Pallas kernels, per_device(): pl.pallas_call(functools.partial(kernel, kvn, tpn, width, gate_heads, up_...  94.9 us
    pallas_call x1, Pallas kernels, per_device(): pl.pallas_call(flush, out_shape=(jax.ShapeDtypeStruct(state_matrix.shape,...  11.3 us

profile of v2, /device:TPU:0, one launch (start us, length us, event | category | flops | bytes accessed | tf_op | source)
XLA Modules:
  0.0 108.1 jit_solution(500875954449830417)
XLA Ops:
  0.6 94.9 %shard_map.192 = (bf16[128,1024]{1,0:T(8,128)(2,1)S(1)}, f32[32,8,128,256]{3,2,1,0:T(8,128)S(1)}, f32[32,8,128]{2,1,0:T(8,128)S(1)}, f32[8,32]{1,0:T(8,128)S(1)}) custom-call(bf16[128,1024]{1,0:T(8,128)(2,1)} %x_hbm.1, bf16[8,128]{1,0:T(8,128)(2,1)} %bitcast.13, bf16[1024,1024]{1,0:T(8,128)(2,1)} %q_hbm.1, bf16[1024,1024]{1,0:T(8,128)(2,1)} %k_hbm.1, ...), custom_call_target="tpu_custom_call" | custom-call | tf_op jit(solution)/shard_map/pallas_call | solution.py:935
  95.6 11.3 %shard_map.193 = (f32[32,8,128,256]{3,2,1,0:T(8,128)}, bf16[128,1024]{1,0:T(8,128)(2,1)}) custom-call(f32[32,8,128,256]{3,2,1,0:T(8,128)S(1)} %get-tuple-element.10.refs_0_, bf16[128,1024]{1,0:T(8,128)(2,1)S(1)} %get-tuple-element.11.refs_1_), custom_call_target="tpu_custom_call" | custom-call | tf_op jit(solution)/shard_map/pallas_call | solution.py:971
  106.9 0.6 copy.24
  107.5 0.7 copy.23

commit v3 on v2

--- a/solution.py
+++ b/solution.py
@@ -174,15 +174,15 @@
     def qkv_loads(h):
         found = []
         at = 0
-        for i, (ref, extent) in enumerate(((q_hbm, dqk), (k_hbm, dqk), (v_hbm, dv))):
+        for ref, extent in ((q_hbm, dqk), (k_hbm, dqk), (v_hbm, dv)):
             src = ref.at[:, pl.ds(pl.multiple_of(h * extent, extent), extent)]
-            found.append(pltpu.make_async_copy(src, weights.at[gate_chunks + h, :, pl.ds(at, extent)], w_sem.at[gate_chunks + h, i]))
+            found.append(pltpu.make_async_copy(src, weights.at[gate_chunks + h, :, pl.ds(at, extent)], w_sem.at[gate_chunks + h]))
             at += extent
         return found
 
     def gate_load(c):
         src = o_hbm.at[:, pl.ds(pl.multiple_of(c * gate_width, gate_width), gate_width)]
-        return pltpu.make_async_copy(src, weights.at[c, :, pl.ds(0, gate_width)], w_sem.at[c, 0])
+        return pltpu.make_async_copy(src, weights.at[c, :, pl.ds(0, gate_width)], w_sem.at[c])
 
     for c in range(min(1, gate_chunks)):
         gate_load(c).start()
@@ -239,6 +239,9 @@
     for copy in gate_copies:
         copy.start()
 
+    def kind(c):
+        return jnp.minimum(c // gate_chunks, 1)
+
     def block(buf, c, d, wide):
         if wide == width:
             return buf.at[c, d]
@@ -247,12 +250,12 @@
     def outer_sends(c, wide):
         found = []
         dests = [d for _, _, d in outside()] + [partner]
-        for i, d in enumerate(dests):
+        for d in dests:
             found.append(
                 remote(
                     block(part_send, c, d, wide),
                     block(pair_recv, c, d, wide),
-                    pair_ss.at[c, i],
+                    pair_ss.at[kind(c)],
                     pair_rs.at[c, d],
                     "kv",
                     partner,
@@ -264,7 +267,7 @@
         return remote(
             block(part_send, c, partner, wide),
             block(pair_recv, c, partner, wide),
-            pair_ss.at[c, 0],
+            pair_ss.at[kind(c)],
             pair_rs.at[c, partner],
             "kv",
             partner,
@@ -298,8 +301,8 @@
     lax.fori_loop(0, gate_chunks, gate_project, 0)
 
     def qkv_project(h, carry):
-        for copy in qkv_loads(h):
-            copy.wait()
+        whole = weights.at[gate_chunks + h]
+        pltpu.make_async_copy(up_hbm.at[:, pl.ds(0, width)], whole, w_sem.at[gate_chunks + h]).wait()
         state_load(h).start()
         project(gate_chunks + h, width)
         return carry
@@ -371,7 +374,7 @@
                     remote(
                         block(pair_recv, c, d, wide),
                         block(cross_recv, c, slot, wide),
-                        cross_ss.at[c, (jj - 1) * 2 + b],
+                        cross_ss.at[kind(c)],
                         cross_rs.at[c, slot],
                         "kv",
                         d,
@@ -382,7 +385,7 @@
 
     def combine(c, wide):
         for d, copy in cross_sends(c, wide):
-            arrived(block(pair_recv, c, d, wide), pair_rs.at[c, d], pair_ss.at[c, 0])
+            arrived(block(pair_recv, c, d, wide), pair_rs.at[c, d], pair_ss.at[0])
             cols = pl.ds(0, wide)
             both = part_send[c, d, :, cols].astype(F32) + pair_recv[c, d, :, cols].astype(F32)
             pair_recv[c, d, :, cols] = both.astype(BF16)
@@ -430,9 +433,9 @@
                         copy.start()
 
     def summed(c, wide):
-        arrived(block(pair_recv, c, me, wide), pair_rs.at[c, me], pair_ss.at[c, 0])
+        arrived(block(pair_recv, c, me, wide), pair_rs.at[c, me], pair_ss.at[0])
         for i in range(npairs - 1):
-            arrived(block(cross_recv, c, i, wide), cross_rs.at[c, i], pair_ss.at[c, 0])
+            arrived(block(cross_recv, c, i, wide), cross_rs.at[c, i], pair_ss.at[0])
         found = []
         for g in range(0, wide, LANES):
             cols = pl.ds(g, LANES)
@@ -444,27 +447,30 @@
 
     last = heads - 1
 
+    def final(h):
+        return (h + 1) // heads
+
     def own_sends(h):
         src = merged_all.at[h, me]
         return [
-            remote(src, src, ag_ss.at[h, j - 1], ag_rs.at[h, me], "kv", wrap(j)) for j in range(1, kvn)
+            remote(src, src, ag_ss.at[final(h)], ag_rs.at[h, me], "kv", wrap(j)) for j in range(1, kvn)
         ]
 
     def outer_own(h):
         src = merged_all.at[h, me]
-        return remote(src, src, ag_ss.at[h, 0], ag_rs.at[h, me], "kv", partner)
+        return remote(src, src, ag_ss.at[final(h)], ag_rs.at[h, me], "kv", partner)
 
     def relay_sends(h):
         src = merged_all.at[h, partner]
         return [
-            remote(src, src, relay_ss.at[h, (jj - 1) * 2 + b], ag_rs.at[h, partner], "kv", d)
+            remote(src, src, relay_ss.at[0], ag_rs.at[h, partner], "kv", d)
             for jj, b, d in outside()
         ]
 
     def relay(h):
         @pl.when(leader)
         def _():
-            arrived(merged_all.at[h, partner], ag_rs.at[h, partner], ag_ss.at[h, 0])
+            arrived(merged_all.at[h, partner], ag_rs.at[h, partner], ag_ss.at[0])
             for copy in relay_sends(h):
                 copy.start()
 
@@ -486,11 +492,11 @@
     def out_project(batch, first):
         for h in batch:
             for _, _, d in outside():
-                arrived(merged_all.at[h, d], ag_rs.at[h, d], ag_ss.at[h, 0])
+                arrived(merged_all.at[h, d], ag_rs.at[h, d], ag_ss.at[0])
 
             @pl.when(jnp.logical_or(outer, h == last))
             def _(h=h):
-                arrived(merged_all.at[h, partner], ag_rs.at[h, partner], ag_ss.at[h, 0])
+                arrived(merged_all.at[h, partner], ag_rs.at[h, partner], ag_ss.at[0])
 
         for b in range(out_cols):
 
@@ -639,7 +645,7 @@
     per_slot = width // up_width
 
     def outer_up(c):
-        return remote(upb.at[0, c], upb.at[1, c], up_ss.at[c], up_rs.at[c], "kv", partner)
+        return remote(upb.at[0, c], upb.at[1, c], up_ss.at[0], up_rs.at[c], "kv", partner)
 
     def up_body(c, carry):
         slot = out_blocks + c // per_slot
@@ -668,15 +674,15 @@
             head = 2 * other + 1 - (2 * other) // npairs
             slot = npairs - jj - 1
             found.append(
-                remote(upb.at[1, c], up_cross.at[c, slot], upx_ss.at[c, jj - 1], upx_rs.at[c, slot], "kv", head)
+                remote(upb.at[1, c], up_cross.at[c, slot], upx_ss.at[0], upx_rs.at[c, slot], "kv", head)
             )
         return found
 
     def hidden_send(c):
-        return remote(upb.at[0, c], upb.at[1, c], hid_ss.at[c], hid_rs.at[c], "kv", partner)
+        return remote(upb.at[0, c], upb.at[1, c], hid_ss.at[0], hid_rs.at[c], "kv", partner)
 
     def up_combine(c):
-        arrived(upb.at[1, c], up_rs.at[c], up_ss.at[c])
+        arrived(upb.at[1, c], up_rs.at[c], up_ss.at[0])
         both = upb[0, c].astype(F32) + upb[1, c].astype(F32)
         upb[1, c] = both.astype(BF16)
         for copy in up_cross_sends(c):
@@ -684,7 +690,7 @@
 
     def up_finish(c):
         for i in range(npairs - 1):
-            arrived(up_cross.at[c, i], upx_rs.at[c, i], up_ss.at[c])
+            arrived(up_cross.at[c, i], upx_rs.at[c, i], up_ss.at[0])
         for g in range(0, up_width, LANES):
             cols = pl.ds(g, LANES)
             val = upb[1, c, :, cols].astype(F32)
@@ -727,7 +733,7 @@
     @pl.when(outer)
     def _():
         def tick(c, carry):
-            arrived(upb.at[1, c], hid_rs.at[c], up_ss.at[c])
+            arrived(upb.at[1, c], hid_rs.at[c], up_ss.at[0])
             down_project(c, 1)
             return carry
 
@@ -747,57 +753,42 @@
     for copy in sent + gate_copies + sq_copies:
         copy.wait_send()
 
-    def drain(c, wide):
-        @pl.when(outer)
-        def _():
-            for copy in outer_sends(c, wide):
-                copy.wait_send()
-
-        @pl.when(leader)
-        def _():
-            inner_send(c, wide).wait_send()
-            for _, copy in cross_sends(c, wide):
-                copy.wait_send()
-
-    def drain_gate(c, carry):
-        drain(c, gate_width)
-        return carry
-
-    def drain_qkv(h, carry):
-        drain(gate_chunks + h, width)
-        direct = jnp.logical_or(leader, h == last)
-
-        @pl.when(direct)
-        def _():
-            for copy in own_sends(h):
-                copy.wait_send()
-
-        @pl.when(jnp.logical_not(direct))
-        def _():
-            outer_own(h).wait_send()
-
-        @pl.when(jnp.logical_and(leader, h < last))
-        def _():
-            for copy in relay_sends(h):
-                copy.wait_send()
-
-        return carry
-
-    def drain_up(c, carry):
-        @pl.when(outer)
-        def _():
-            outer_up(c).wait_send()
-
-        @pl.when(leader)
-        def _():
-            for copy in up_cross_sends(c) + [hidden_send(c)]:
-                copy.wait_send()
-
-        return carry
-
-    lax.fori_loop(0, heads, drain_qkv, 0)
-    lax.fori_loop(0, gate_chunks, drain_gate, 0)
-    lax.fori_loop(0, up_chunks, drain_up, 0)
+    def sent_all(ref, ssem):
+        remote(ref, ref, ssem, pair_rs.at[0, 0], "kv", partner).wait_send()
+
+    def projections(n):
+        gate_part = part_send.at[pl.ds(0, gate_chunks), pl.ds(0, n), :, pl.ds(0, gate_width)]
+        return gate_part, part_send.at[pl.ds(gate_chunks, heads), pl.ds(0, n)]
+
+    def readouts(first, count, n):
+        return merged_all.at[pl.ds(first, count), pl.ds(0, n)]
+
+    others = kvn - 1
+    beyond = kvn - 2
+
+    @pl.when(outer)
+    def _():
+        for i, ref in enumerate(projections(others)):
+            sent_all(ref, pair_ss.at[i])
+        if last:
+            sent_all(readouts(0, last, 1), ag_ss.at[0])
+        sent_all(readouts(last, 1, others), ag_ss.at[1])
+        sent_all(upb.at[0], up_ss.at[0])
+
+    @pl.when(leader)
+    def _():
+        for i, ref in enumerate(projections(1)):
+            sent_all(ref, pair_ss.at[i])
+        if last:
+            sent_all(readouts(0, last, others), ag_ss.at[0])
+        sent_all(readouts(last, 1, others), ag_ss.at[1])
+        if beyond:
+            for i, ref in enumerate(projections(beyond)):
+                sent_all(ref, cross_ss.at[i])
+            if last:
+                sent_all(readouts(0, last, beyond), relay_ss.at[0])
+            sent_all(up_cross, upx_ss.at[0])
+        sent_all(upb.at[0], hid_ss.at[0])
 
 
 def flush(*refs):
@@ -903,18 +894,18 @@
         V((2, up_chunks, total, up_width), BF16),
         V((up_chunks, np1, total, up_width), BF16),
         dma((9,)),
-        dma((chunks, 3)),
+        dma((chunks,)),
         dma((slots2,)),
         dma((1,)),
         dma((heads,)),
         dma((k1,)),
         dma((k1,)),
-        dma((chunks, k1)),
+        dma((2,)),
         dma((chunks, kvn)),
-        dma((chunks, 2 * np1)),
+        dma((2,)),
         dma((chunks, np1)),
-        dma((heads, k1)),
-        dma((heads, 2 * np1)),
+        dma((2,)),
+        dma((1,)),
         dma((heads, kvn)),
         dma((2, PIECES)),
         dma((2, PIECES)),
@@ -924,11 +915,11 @@
         dma((2, PIECES)),
         dma((k1,)),
         dma((k1,)),
+        dma((1,)),
         dma((up_chunks,)),
-        dma((up_chunks,)),
+        dma((1,)),
         dma((up_chunks, np1)),
-        dma((up_chunks, np1)),
-        dma((up_chunks,)),
+        dma((1,)),
         dma((up_chunks,)),
     ]
     state_bytes = state_matrix.size * 4

time: 108 us -> 106 us (0.981)
  Pallas kernels: 106 us -> 104 us
    pallas_call x1, Pallas kernels: 94.9 us -> 93.2 us  [per_device(): pl.pallas_call(functools.partial(kernel, kvn, tpn, width, gate_heads, up_...]
where the time goes in v3:
time: 106 us
  Pallas kernels  104 us (98%)
  local copies, waits for them, and re-layouts  1.25 us (1%)
    pallas_call x1, Pallas kernels, per_device(): pl.pallas_call(functools.partial(kernel, kvn, tpn, width, gate_heads, up_...  93.2 us
    pallas_call x1, Pallas kernels, per_device(): pl.pallas_call(flush, out_shape=(jax.ShapeDtypeStruct(state_matrix.shape,...  11.3 us

profile of v3, /device:TPU:0, one launch (start us, length us, event | category | flops | bytes accessed | tf_op | source)
XLA Modules:
  0.0 106.3 jit_solution(188907428939436067)
XLA Ops:
  0.6 93.2 %shard_map.192 = (bf16[128,1024]{1,0:T(8,128)(2,1)S(1)}, f32[32,8,128,256]{3,2,1,0:T(8,128)S(1)}, f32[32,8,128]{2,1,0:T(8,128)S(1)}, f32[8,32]{1,0:T(8,128)S(1)}) custom-call(bf16[128,1024]{1,0:T(8,128)(2,1)} %x_hbm.1, bf16[8,128]{1,0:T(8,128)(2,1)} %bitcast.13, bf16[1024,1024]{1,0:T(8,128)(2,1)} %q_hbm.1, bf16[1024,1024]{1,0:T(8,128)(2,1)} %k_hbm.1, ...), custom_call_target="tpu_custom_call" | custom-call | tf_op jit(solution)/shard_map/pallas_call | solution.py:926
  93.8 11.3 %shard_map.193 = (f32[32,8,128,256]{3,2,1,0:T(8,128)}, bf16[128,1024]{1,0:T(8,128)(2,1)}) custom-call(f32[32,8,128,256]{3,2,1,0:T(8,128)S(1)} %get-tuple-element.10.refs_0_, bf16[128,1024]{1,0:T(8,128)(2,1)S(1)} %get-tuple-element.11.refs_1_), custom_call_target="tpu_custom_call" | custom-call | tf_op jit(solution)/shard_map/pallas_call | solution.py:962
  105.1 0.6 copy.24
  105.7 0.7 copy.23
